TPU v7x, 32 devices: a whole 2x2x4 slice. The times are simulated.
32 devices in a mesh: ep: 8 (over z, x), tp: 4 (over y, core).
Axes of the slice: x: 2, y: 2, z: 4, core: 2. Of those that a mesh axis runs over, the one named last changes fastest.
Arguments:
- tokens: bfloat16 [256, 2048], P('ep'), may hold values from -6 to 6
- lengths: int32 [256], P('ep'), may hold values from 128 to 1024, as said below
- cache_keys: bfloat16 [256, 1024, 1024], P('ep', None, 'tp'), may hold values from -140 to 140
- cache_values: bfloat16 [256, 1024, 1024], P('ep', None, 'tp'), may hold values from -6 to 6
- attn_gain: float32 [2048], replicated, may hold values from 0.1 to 1.9
- q_first_w: bfloat16 [2048, 512], P(None, 'tp'), may hold values from -0.19921875 to 0.19921875
- q_second_w: bfloat16 [2048, 512], P(None, 'tp'), may hold values from -0.19921875 to 0.19921875
- k_first_w: bfloat16 [2048, 512], P(None, 'tp'), may hold values from -0.125 to 0.125
- k_second_w: bfloat16 [2048, 512], P(None, 'tp'), may hold values from -0.125 to 0.125
- value_w: bfloat16 [2048, 1024], P(None, 'tp'), may hold values from -0.125 to 0.125
- mix_lambda: float32 [8], P('tp'), may hold values from 0.3 to 0.8
- head_gain: float32 [128], replicated, may hold values from 0.1 to 1.9
- out_w: bfloat16 [1024, 2048], P('tp'), may hold values from -0.09375 to 0.09375
- ffn_gain: float32 [2048], replicated, may hold values from 0.1 to 1.9
- routes: int32 [256, 4], P('ep'), may hold values from 0 to 31, all different within a row; in each aligned block of 32 rows (0 to 31, 32 to 63, ...) at most 8 rows name the same one
- route_logits: float32 [256, 4], P('ep'), may hold values from -4 to 4
- gate_w: bfloat16 [32, 2048, 1024], P('ep', None, 'tp'), may hold values from -0.34960938 to 0.34960938
- up_w: bfloat16 [32, 2048, 1024], P('ep', None, 'tp'), may hold values from -0.34960938 to 0.34960938
- down_w: bfloat16 [32, 1024, 2048], P('ep', None, 'tp'), may hold values from -0.125 to 0.125
Outputs:
- mixed: bfloat16 [256, 2048], P('ep', 'tp')
Inputs may be any that keep to these rules, and one draw needn't show every extreme that they name: `lengths`: at least 128 positions; among the 32 sequences of each index of ep one holds exactly 1024. `routes`: each row names 4 different experts; within the rows of one device no expert is named more than 8 times, a bound that some block reaches.
All inputs are finite; a program needn't handle non-finite values.
Results may differ from a plain program's by a relative error of at most 0.015.
Values may be sent and summed in bfloat16 or wider, within the bound.
A program may use at most 128 MiB of HBM per device.

v0:
```python
import functools

import jax
import jax.numpy as jnp
from jax import lax
from jax.experimental import pallas as pl
from jax.experimental.pallas import tpu as pltpu
from jax.sharding import PartitionSpec as P

EPS = 1e-06
LIMIT = 7.0
ALPHA = 1.702
PIECE = 128
GROUP = 8
VMEM_BYTES = 67043328
F32 = jnp.float32
BF16 = jnp.bfloat16


def attend_kernel(
    heads,
    lam_ref,
    lengths_hbm,
    tokens_hbm,
    again_hbm,
    hgain_hbm,
    keys_hbm,
    values_hbm,
    q1_hbm,
    q2_hbm,
    k1_hbm,
    k2_hbm,
    vw_hbm,
    ow_hbm,
    part_ref,
    kbuf,
    vbuf,
    q1_v,
    q2_v,
    k1_v,
    k2_v,
    vw_v,
    ow_v,
    queries,
    own_keys,
    new_values,
    attended,
    lengths_ref,
    tokens_ref,
    again_ref,
    hgain_ref,
    ksem,
    vsem,
    wsem,
    ssem,
):
    smalls = ((lengths_hbm, lengths_ref), (tokens_hbm, tokens_ref), (again_hbm, again_ref), (hgain_hbm, hgain_ref))
    smalls = [pltpu.make_async_copy(src, dst, ssem.at[i]) for i, (src, dst) in enumerate(smalls)]
    for small in smalls:
        small.start()
    seqs, length, width = kbuf.shape
    head = width // heads
    half = head // 2
    scale = half ** (-0.5)
    weights = ((q1_hbm, q1_v), (q2_hbm, q2_v), (k1_hbm, k1_v), (k2_hbm, k2_v), (vw_hbm, vw_v), (ow_hbm, ow_v))
    loads = [pltpu.make_async_copy(src, dst, wsem.at[i]) for i, (src, dst) in enumerate(weights)]
    for load in loads[:5]:
        load.start()

    def fetch(s):
        rows = pl.multiple_of((lengths_ref[s] + (PIECE - 1)) // PIECE * PIECE, PIECE)
        return (
            pltpu.make_async_copy(keys_hbm.at[s, pl.ds(0, rows)], kbuf.at[s, pl.ds(0, rows)], ksem.at[s]),
            pltpu.make_async_copy(values_hbm.at[s, pl.ds(0, rows)], vbuf.at[s, pl.ds(0, rows)], vsem.at[s]),
        )

    def start(s, carry):
        a, b = fetch(s)
        a.start()
        b.start()
        return carry

    smalls[0].wait()
    lax.fori_loop(0, seqs, start, 0)
    loads[5].start()
    for small in smalls[1:]:
        small.wait()

    wide = tokens_ref[...].astype(F32)
    normed = (
        wide * lax.rsqrt(jnp.mean(wide * wide, axis=-1, keepdims=True) + EPS) * again_ref[...]
    ).astype(BF16)
    for load in loads[:5]:
        load.wait()

    def project(w):
        return jnp.dot(normed, w[...], preferred_element_type=F32).astype(BF16).astype(F32)

    q1, q2, k1, k2 = project(q1_v), project(q2_v), project(k1_v), project(k2_v)
    new_values[...] = project(vw_v)
    zero = jnp.zeros((seqs, half), F32)
    queries[...] = jnp.zeros_like(queries)
    kparts = []
    for h in range(heads):
        cut = slice(h * half, (h + 1) * half)
        kparts += [k1[:, cut], k2[:, cut]]
        for p, q in ((0, q1), (1, q2)):
            parts = [zero] * (2 * heads)
            parts[2 * h + p] = q[:, cut]
            queries[:, 4 * p + h, :] = jnp.concatenate(parts, axis=-1)
    own_keys[...] = jnp.concatenate(kparts, axis=-1)

    position = lax.broadcasted_iota(jnp.int32, (8, length), 1)
    row = lax.broadcasted_iota(jnp.int32, (8, width), 0)
    mine = row == lax.broadcasted_iota(jnp.int32, (8, width), 1) // head
    map_row = lax.broadcasted_iota(jnp.int32, (8, 1), 0)
    lam = jnp.zeros((8, 1), F32)
    for h in range(heads):
        lam = jnp.where(map_row == h, lam_ref[h], lam)
    hgain = jnp.concatenate([hgain_ref[...]] * heads, axis=-1)

    def group_step(g, carry):
        for j in range(GROUP):
            for copy in fetch(g * GROUP + j):
                copy.wait()
        for j in range(GROUP):
            s = g * GROUP + j
            count = lengths_ref[s]
            q = queries[s]
            scores = lax.dot_general(
                q.astype(BF16), kbuf[s], (((1,), (1,)), ((), ())), preferred_element_type=F32
            ) * scale
            own = jnp.sum(q * own_keys[pl.ds(s, 1), :], axis=-1, keepdims=True) * scale
            scores = jnp.where(position < count, scores, -jnp.inf)
            top = jnp.maximum(jnp.max(scores, axis=-1, keepdims=True), own)
            raised = jnp.exp(scores - top)
            own_raised = jnp.exp(own - top)
            total = jnp.sum(raised, axis=-1, keepdims=True) + own_raised
            inv = 1.0 / total
            probs = raised * inv
            own_probs = own_raised * inv
            mixed = (probs - lam * pltpu.roll(probs, 4, 0)).astype(BF16)
            own_b = jnp.broadcast_to(own_probs, (8, 128))
            own_w = (own_b - lam * pltpu.roll(own_b, 4, 0)).astype(BF16).astype(F32)[:, :1]
            pieces = [
                jnp.where(c * PIECE < count, vbuf[s, c * PIECE:(c + 1) * PIECE, :], jnp.zeros((PIECE, width), BF16))
                for c in range(length // PIECE)
            ]
            out = jnp.dot(mixed, jnp.concatenate(pieces, axis=0), preferred_element_type=F32)
            out = out + own_w * new_values[pl.ds(s, 1), :]
            out = jnp.where(mine, out, 0.0)
            mean_sq = jnp.sum(out * out, axis=-1, keepdims=True) * (1.0 / head)
            out = out * lax.rsqrt(mean_sq + EPS)
            attended[pl.ds(s, 1), :] = jnp.sum(out, axis=0, keepdims=True) * hgain
        return carry

    lax.fori_loop(0, seqs // GROUP, group_step, 0)
    loads[5].wait()
    part_ref[...] = jnp.dot(
        attended[...].astype(BF16), ow_v[...], preferred_element_type=F32
    ).reshape(part_ref.shape).astype(part_ref.dtype)


def attend(
    tokens, lengths, cache_keys, cache_values, attn_gain, q1w, q2w, k1w, k2w, vw, lam, hgain, out_w, out_dtype, parts
):
    seqs, length, width = cache_keys.shape
    heads = lam.shape[0]
    vm = pl.BlockSpec(memory_space=pltpu.VMEM)
    anyspace = pl.BlockSpec(memory_space=pltpu.HBM)
    scratch = [pltpu.VMEM(cache_keys.shape, BF16), pltpu.VMEM(cache_values.shape, BF16)]
    scratch += [pltpu.VMEM(w.shape, BF16) for w in (q1w, q2w, k1w, k2w, vw, out_w)]
    scratch += [
        pltpu.VMEM((seqs, 8, width), F32),
        pltpu.VMEM((seqs, width), F32),
        pltpu.VMEM((seqs, width), F32),
        pltpu.VMEM((seqs, width), F32),
        pltpu.SMEM((seqs,), jnp.int32),
        pltpu.VMEM(tokens.shape, BF16),
        pltpu.VMEM((1, tokens.shape[1]), F32),
        pltpu.VMEM((1, hgain.shape[0]), F32),
        pltpu.SemaphoreType.DMA((seqs,)),
        pltpu.SemaphoreType.DMA((seqs,)),
        pltpu.SemaphoreType.DMA((6,)),
        pltpu.SemaphoreType.DMA((4,)),
    ]
    return pl.pallas_call(
        functools.partial(attend_kernel, heads),
        out_shape=jax.ShapeDtypeStruct((parts, seqs // parts, out_w.shape[1]), out_dtype),
        in_specs=[pl.BlockSpec(memory_space=pltpu.SMEM)] + [anyspace] * 12,
        out_specs=vm,
        scratch_shapes=scratch,
        compiler_params=pltpu.CompilerParams(vmem_limit_bytes=VMEM_BYTES),
        name="attend",
    )(
        lam, lengths, tokens, attn_gain.reshape(1, -1), hgain.reshape(1, -1),
        cache_keys, cache_values, q1w, q2w, k1w, k2w, vw, out_w,
    )


MESH = pl.DeviceIdType.MESH


def rms_scale(rows, gain):
    mean_sq = jnp.mean(rows * rows, axis=-1, keepdims=True)
    return rows * lax.rsqrt(mean_sq + EPS) * gain


def exact_dot(a, b):
    return jnp.dot(a, b, precision=lax.Precision.HIGHEST, preferred_element_type=F32)


def where_is(shape, dim):
    return lax.broadcasted_iota(jnp.int32, shape, dim)


def turned_dot(a, b, left, right):
    return lax.dot_general(
        a, b, (((left,), (right,)), ((), ())), precision=lax.Precision.HIGHEST, preferred_element_type=F32
    )


def route_tables(routes, logits, slots, capacity):
    top, seqs = routes.shape
    n = seqs * top
    routes = routes.astype(F32)
    spread = turned_dot(routes, (where_is((top, n), 1) % top == where_is((top, n), 0)).astype(F32), 0, 0)
    row = jnp.sum(jnp.where(where_is((seqs, n), 1) // top == where_is((seqs, n), 0), spread, 0.0), axis=0, keepdims=True)
    owner = (where_is((n, seqs), 0) // top == where_is((n, seqs), 1)).astype(F32)
    pick = where_is((n, top), 0) % top == where_is((n, top), 1)
    col = jnp.sum(jnp.where(pick, turned_dot(owner, routes, 1, 1), 0.0), axis=1, keepdims=True)
    same = row == col
    i, j = where_is((n, n), 0), where_is((n, n), 1)
    rank_col = jnp.sum((same & (j < i)).astype(F32), axis=1, keepdims=True)
    rank_row = jnp.sum((same & (i < j)).astype(F32), axis=0, keepdims=True)
    slot_row = row * capacity + rank_row
    return slot_row, lambda: combine_table(logits, col, rank_col, owner, pick, slots, capacity)


def combine_table(logits, col, rank_col, owner, pick, slots, capacity):
    n, seqs = owner.shape
    top = n // seqs
    slot_col = col * capacity + rank_col
    raised = jnp.exp(logits - jnp.max(logits, axis=0, keepdims=True))
    weights = raised / jnp.sum(raised, axis=0, keepdims=True)
    weight_col = jnp.sum(jnp.where(pick, turned_dot(owner, weights, 1, 1), 0.0), axis=1, keepdims=True)
    hit = where_is((n, slots), 1).astype(F32) == slot_col
    member = (where_is((seqs, n), 1) // top == where_is((seqs, n), 0)).astype(F32)
    combine = exact_dot(member, jnp.where(hit, weight_col, 0.0))
    return combine


def experts_kernel(
    groups,
    parts,
    capacity,
    part_ref,
    tokens_ref,
    fgain_ref,
    routes_ref,
    logits_ref,
    gate_hbm,
    up_hbm,
    down_hbm,
    out_ref,
    gate_v,
    up_v,
    down_v,
    rs_buf,
    wide,
    after,
    kept,
    slot_buf,
    xbuf,
    hbuf,
    resbuf,
    ret,
    combine_v,
    wsem,
    rs_s,
    rs_r,
    sl_s,
    sl_r,
    k_s,
    k_r,
    xe_s,
    xe_r,
    xy_s,
    xy_r,
    xc_s,
    xc_r,
    xd_s,
    xd_r,
    hy_s,
    hy_r,
    hc_s,
    hc_r,
    hd_s,
    hd_r,
    re_s,
    re_r,
):
    e, t = lax.axis_index("ep"), lax.axis_index("tp")
    owned = gate_v.shape[0]
    rows, width = after.shape
    columns = out_ref.shape[1]
    seqs = rows * parts
    top = routes_ref.shape[0]
    n = seqs * top
    block = owned * capacity
    twin = t + 1 - 2 * lax.rem(t, 2)
    across = lax.rem(t + 2, parts)

    loads = []
    for j in range(owned):
        for i, (src, dst) in enumerate(((gate_hbm, gate_v), (up_hbm, up_v), (down_hbm, down_v))):
            loads.append(pltpu.make_async_copy(src.at[j], dst.at[j], wsem.at[3 * j + i]))
            loads[-1].start()

    barrier = pltpu.get_barrier_semaphore()
    for k in range(1, parts):
        pl.semaphore_signal(barrier, inc=1, device_id=(e, lax.rem(t + k, parts)), device_id_type=MESH)
    for k in range(1, groups):
        pl.semaphore_signal(barrier, inc=1, device_id=(lax.rem(e + k, groups), t), device_id_type=MESH)
    pl.semaphore_wait(barrier, parts + groups - 2)

    sent = []

    def send(src, dst, s_sem, r_sem, device):
        copy = pltpu.make_async_remote_copy(
            src_ref=src, dst_ref=dst, send_sem=s_sem, recv_sem=r_sem, device_id=device, device_id_type=MESH
        )
        copy.start()
        sent.append(copy)
        return copy

    scatter = []
    for k in range(1, parts):
        peer = lax.rem(t + k, parts)
        scatter.append(send(part_ref.at[peer], rs_buf.at[k - 1], rs_s.at[k - 1], rs_r.at[k - 1], (e, peer)))

    slot_row, later = route_tables(routes_ref[...], logits_ref[...], groups * block, capacity)
    slot_buf[e] = jnp.broadcast_to(slot_row, (8, n))
    tables = []
    for k in range(1, groups):
        tables.append(
            send(slot_buf.at[e], slot_buf.at[e], sl_s.at[k - 1], sl_r.at[k - 1], (lax.rem(e + k, groups), t))
        )
    wide[...] = tokens_ref[...].astype(F32).reshape(parts, rows, width)
    total = part_ref[t].astype(F32)
    for k in range(1, parts):
        scatter[k - 1].wait_recv()
        total = total + rs_buf[k - 1].astype(F32)
    total = wide[t] + total
    after[...] = total
    xbuf[e, t] = rms_scale(total, fgain_ref[...]).astype(BF16)

    inner = 2 if groups % 2 == 0 else 1
    outer = groups // inner
    place_out, place_in = e // inner, lax.rem(e, inner)
    gather = []
    for m in range(1, outer):
        peer = lax.rem(place_out + m, outer) * inner + place_in
        gather.append(send(xbuf.at[e, t], xbuf.at[e, t], xe_s.at[m - 1], xe_r.at[m - 1], (peer, t)))
    side = place_out * inner + inner - 1 - place_in
    turns = [(0, 0)]
    for m in range(1, outer):
        turns += [(m, 0)] + [(m - 1, 1)] * (inner - 1)
    turns += [(outer - 1, 1)] * (inner - 1)
    passed = [None] * outer
    sources = []
    far, near, relay = [], [], []
    for k, (m, other) in enumerate(turns):
        line_in = inner - 1 - place_in if other else place_in
        source = lax.rem(place_out - m + outer, outer) * inner + line_in
        sources.append(source)
        if other:
            passed[m].wait_recv()
        elif m:
            gather[m - 1].wait_recv()
        if inner > 1 and not other:
            i = outer - 1 + m
            passed[m] = send(xbuf.at[source, t], xbuf.at[source, t], xe_s.at[i], xe_r.at[i], (side, t))
        mine = xbuf.at[source, t]
        far.append(send(mine, mine, xy_s.at[k], xy_r.at[k], (e, across)))
        near.append(send(mine, mine, xc_s.at[k], xc_r.at[k], (e, twin)))
        if k == 0:
            combine_v[...] = later()
            keep = []
            kept[t] = after[:, pl.ds(pl.multiple_of(t * columns, columns), columns)]
            for q in range(1, parts):
                peer = lax.rem(t + q, parts)
                view = after.at[:, pl.ds(pl.multiple_of(peer * columns, columns), columns)]
                keep.append(send(view, kept.at[t], k_s.at[q - 1], k_r.at[q - 1], (e, peer)))
    for table in tables:
        table.wait_recv()
    base = e * block
    local = (where_is((block, n), 0) + base).astype(F32)
    place = []
    for b in range(groups):
        chosen = (slot_buf[b][:1, :] == local).astype(BF16)
        spot = (where_is((n, groups * seqs), 1) == where_is((n, groups * seqs), 0) // top + b * seqs).astype(BF16)
        placed = jnp.dot(chosen, spot, preferred_element_type=F32)
        place.append(placed.reshape(owned, 1, capacity, groups * seqs))
    dispatch = jnp.concatenate(place, axis=1).reshape(groups * block, groups * seqs).astype(BF16)
    for k, source in enumerate(sources):
        far[k].wait_recv()
        theirs = xbuf.at[source, across]
        relay.append(send(theirs, theirs, xd_s.at[k], xd_r.at[k], (e, twin)))
    for copy in near + relay:
        copy.wait_recv()

    everything = xbuf[...].astype(F32).reshape(groups * seqs, width).astype(BF16)
    lines = jnp.dot(dispatch, everything, preferred_element_type=F32).astype(BF16)
    per = groups * capacity
    hfar, hnear = [], []
    for j in range(owned):
        for i in range(2):
            loads[3 * j + i].wait()
        line = lines[j * per:(j + 1) * per]
        gate = jnp.minimum(jnp.dot(line, gate_v[j], preferred_element_type=F32), LIMIT)
        up = jnp.clip(jnp.dot(line, up_v[j], preferred_element_type=F32), -LIMIT, LIMIT)
        hbuf[j, t] = ((up + 1.0) * gate * jax.nn.sigmoid(ALPHA * gate)).astype(BF16)
        mine = hbuf.at[j, t]
        hfar.append(send(mine, mine, hy_s.at[j], hy_r.at[j], (e, across)))
        hnear.append(send(mine, mine, hc_s.at[j], hc_r.at[j], (e, twin)))
    hrelay = []
    for j in range(owned):
        hfar[j].wait_recv()
        theirs = hbuf.at[j, across]
        hrelay.append(send(theirs, theirs, hd_s.at[j], hd_r.at[j], (e, twin)))
    deep = hbuf.shape[3]
    back = []
    for j in range(owned):
        hnear[j].wait_recv()
        hrelay[j].wait_recv()
        loads[3 * j + 2].wait()
        result = jnp.zeros((per, columns), F32)
        for q in range(parts):
            result += jnp.dot(hbuf[j, q], down_v[j, q * deep:(q + 1) * deep, :], preferred_element_type=F32)
        resbuf[j] = result.reshape(groups, capacity, columns).astype(BF16)
        for k in range(1, groups):
            peer = lax.rem(e + k, groups)
            i = j * (groups - 1) + k - 1
            back.append(send(resbuf.at[j, peer], ret.at[e, j], re_s.at[i], re_r.at[i], (peer, t)))
        ret[e, j] = resbuf[j, e]
    for copy in keep + back:
        copy.wait_recv()
    moe = exact_dot(combine_v[...], ret[...].astype(F32).reshape(groups * block, columns))
    out_ref[...] = (kept[...].reshape(seqs, columns) + moe).astype(out_ref.dtype)
    for copy in sent:
        copy.wait_send()


def experts(part, tokens, ffn_gain, routes, logits, gate_w, up_w, down_w, groups, parts, capacity):
    seqs, width = tokens.shape
    rows = seqs // parts
    owned, _, deep = gate_w.shape
    columns = down_w.shape[2]
    per = groups * capacity
    vm = pl.BlockSpec(memory_space=pltpu.VMEM)
    anyspace = pl.BlockSpec(memory_space=pltpu.HBM)
    dma = lambda count: [pltpu.SemaphoreType.DMA((count,)), pltpu.SemaphoreType.DMA((count,))]
    scratch = [
        pltpu.VMEM(gate_w.shape, BF16),
        pltpu.VMEM(up_w.shape, BF16),
        pltpu.VMEM(down_w.shape, BF16),
        pltpu.VMEM((parts - 1, rows, width), BF16),
        pltpu.VMEM((parts, rows, width), F32),
        pltpu.VMEM((rows, width), F32),
        pltpu.VMEM((parts, rows, columns), F32),
        pltpu.VMEM((groups, 8, routes.size), F32),
        pltpu.VMEM((groups, parts, rows, width), BF16),
        pltpu.VMEM((owned, parts, per, deep), BF16),
        pltpu.VMEM((owned, groups, capacity, columns), BF16),
        pltpu.VMEM((groups, owned, capacity, columns), BF16),
        pltpu.VMEM((seqs, owned * per), F32),
        pltpu.SemaphoreType.DMA((3 * owned,)),
    ]
    scratch += dma(parts - 1) + dma(groups - 1) + dma(parts - 1) + dma(groups - 1)
    scratch += dma(groups) * 3 + dma(owned) * 3 + dma(owned * (groups - 1))
    return pl.pallas_call(
        functools.partial(experts_kernel, groups, parts, capacity),
        out_shape=jax.ShapeDtypeStruct((seqs, columns), BF16),
        in_specs=[vm] * 5 + [anyspace] * 3,
        out_specs=vm,
        scratch_shapes=scratch,
        compiler_params=pltpu.CompilerParams(
            collective_id=0, has_side_effects=True, vmem_limit_bytes=VMEM_BYTES
        ),
        name="experts",
    )(part, tokens, ffn_gain.reshape(1, -1), routes.T, logits.T, gate_w, up_w, down_w)


def slot_tables(routes, weights, expert_ids, capacity):
    blocks, seqs, top = routes.shape
    flat = routes.reshape(blocks, seqs * top)
    order = jnp.arange(seqs * top, dtype=jnp.int32)
    same = (flat[:, None, :] == flat[:, :, None]) & (order[None, None, :] < order[None, :, None])
    rank = jnp.sum(same.astype(jnp.int32), axis=2)
    match = flat[:, :, None] == expert_ids[None, None, :]
    hit = rank[:, :, None] == jnp.arange(capacity, dtype=jnp.int32)[None, None, :]
    table = (match[:, :, :, None] & hit[:, :, None, :]).astype(jnp.float32)
    table = table.reshape(blocks, seqs, top, expert_ids.shape[0], capacity)
    dispatch = jnp.sum(table, axis=2)
    combine = jnp.sum(table * weights[:, :, :, None, None], axis=2)
    return (dispatch, combine)


def run_experts(buffer, gate_w, up_w, down_w):
    gate = jnp.einsum("bjcd,jdf->bjcf", buffer, gate_w, preferred_element_type=jnp.float32)
    up = jnp.einsum("bjcd,jdf->bjcf", buffer, up_w, preferred_element_type=jnp.float32)
    bound_gate = jnp.minimum(gate, LIMIT)
    bound_up = jnp.clip(up, -LIMIT, LIMIT)
    hidden = ((bound_up + 1.0) * bound_gate * jax.nn.sigmoid(ALPHA * bound_gate)).astype(
        jnp.bfloat16
    )
    total = jnp.einsum(
        "bjcf,jfd->bjcd",
        lax.all_gather(hidden, "tp", axis=3, tiled=True),
        down_w,
        preferred_element_type=jnp.float32,
    )
    return total.astype(jnp.bfloat16)


def per_device(
    tokens,
    lengths,
    cache_keys,
    cache_values,
    attn_gain,
    q_first_w,
    q_second_w,
    k_first_w,
    k_second_w,
    value_w,
    mix_lambda,
    head_gain,
    out_w,
    ffn_gain,
    routes,
    route_logits,
    gate_w,
    up_w,
    down_w,
):
    groups, parts = lax.axis_size("ep"), lax.axis_size("tp")
    owned = gate_w.shape[0]
    seqs, top = routes.shape
    capacity = max(2, 2 * seqs * top // (owned * groups))
    fused = parts == 4 and seqs % (8 * parts) == 0 and capacity % 8 == 0 and seqs * top % 128 == 0
    partial_value = attend(
        tokens,
        lengths,
        cache_keys,
        cache_values,
        attn_gain,
        q_first_w,
        q_second_w,
        k_first_w,
        k_second_w,
        value_w,
        mix_lambda,
        head_gain,
        out_w,
        BF16 if fused else F32,
        parts if fused else 1,
    )
    if fused:
        return experts(
            partial_value, tokens, ffn_gain, routes, route_logits, gate_w, up_w, down_w, groups, parts, capacity
        )
    partial_value = partial_value.reshape(tokens.shape)
    wide = tokens.astype(F32)
    columns = wide.shape[1] // lax.axis_size("tp")
    start = lax.axis_index("tp") * columns
    summed = lax.psum(partial_value, "tp")
    after = wide + summed
    full_in = rms_scale(after, ffn_gain).astype(jnp.bfloat16)
    kept = lax.dynamic_slice_in_dim(after, start, columns, 1)
    weights = jax.nn.softmax(route_logits, axis=-1)
    expert_ids = jnp.arange(owned * groups, dtype=jnp.int32)
    dispatch, combine = slot_tables(routes[None], weights[None], expert_ids, capacity)
    buffer = jnp.einsum(
        "bsjc,bsd->bjcd",
        dispatch.astype(jnp.bfloat16),
        full_in[None],
        preferred_element_type=jnp.float32,
    ).astype(jnp.bfloat16)
    buffer = buffer.reshape(groups, owned, capacity, -1)
    arrived = lax.all_to_all(buffer, "ep", split_axis=0, concat_axis=0, tiled=True)
    results = run_experts(arrived, gate_w, up_w, down_w)
    returned = lax.all_to_all(results, "ep", split_axis=0, concat_axis=0, tiled=True).reshape(
        1, groups * owned, capacity, -1
    )
    moe = jnp.einsum(
        "bsjc,bjcd->bsd", combine, returned.astype(jnp.float32), precision=lax.Precision.HIGHEST
    )[0]
    return (kept + moe).astype(jnp.bfloat16)


def solution(mesh):
    return jax.shard_map(
        per_device,
        mesh=mesh,
        in_specs=(
            P("ep", None),
            P("ep"),
            P("ep", None, "tp"),
            P("ep", None, "tp"),
            P(),
            P(None, "tp"),
            P(None, "tp"),
            P(None, "tp"),
            P(None, "tp"),
            P(None, "tp"),
            P("tp"),
            P(),
            P("tp", None),
            P(),
            P("ep", None),
            P("ep", None),
            P("ep", None, "tp"),
            P("ep", None, "tp"),
            P("ep", None, "tp"),
        ),
        out_specs=P("ep", "tp"),
        check_vma=False,
    )
```

profile of v0, /device:TPU:0, one launch (start us, length us, event | category | flops | bytes accessed | tf_op | source)
XLA Modules:
  0.0 63.7 jit_solution(9305522874807909427)
XLA Ops:
  0.0 22.6 %attend.1.part_ref = bf16[4,8,2048]{2,1,0:T(8,128)(2,1)} custom-call(f32[2]{0:T(128)} %lam_ref.1, s32[32]{0:T(128)} %lengths_hbm.1, bf16[32,2048]{1,0:T(8,128)(2,1)} %tokens_ref.1, f32[1,2048]{1,0:T(1,128)} %bitcast.5, f32[1,128]{1,0:T(1,128)} %bitcast.9, bf16[32,1024,256]{2,1,0:T(8,128)(2,1)} %keys_hbm.1, bf16[32,1024,256]{2,1,0:T(8,128)(2,1)} %values_hbm.1, ...), custom_call_target="tpu_custom_call" | custom-call | tf_op jit(solution)/shard_map/attend/pallas_call | solution.py:187
  22.6 39.7 %experts.1 = bf16[32,512]{1,0:T(8,128)(2,1)} custom-call(bf16[4,8,2048]{2,1,0:T(8,128)(2,1)} %attend.1.part_ref, bf16[32,2048]{1,0:T(8,128)(2,1)} %tokens_ref.1, f32[1,2048]{1,0:T(1,128)} %bitcast.6, s32[4,32]{1,0:T(4,128)} %bitcast.7, f32[4,32]{1,0:T(4,128)} %bitcast.8, bf16[4,2048,256]{2,1,0:T(8,128)(2,1)} %gate_hbm.1, bf16[4,2048,256]{2,1,0:T(8,128)(2,1)} %up_hbm.1, ...), custom_call_target="tpu_custom_call" | custom-call | tf_op jit(solution)/shard_map/experts/pallas_call | solution.py:482
  62.3 1.4 %copy.21 = bf16[32,512]{1,0:T(8,128)(2,1)} copy(bf16[32,512]{1,0:T(8,128)(2,1)} %experts.1) | data formatting | bytes 65536
where the time goes:
time: 63.7 us
  Pallas kernels  62.3 us (98%)
  local copies, waits for them, and re-layouts  1.38 us (2%)
    pallas_call x1, Pallas kernels, experts(): pl.pallas_call(functools.partial(experts_kernel, groups, parts, capacity)...  39.7 us
    pallas_call x1, Pallas kernels, attend(): pl.pallas_call(functools.partial(attend_kernel, heads), out_shape=jax.Sha...  22.6 us
    unnamed x1, local copies, waits for them, and re-layouts  1.38 us

commit v1 on v0

--- a/solution.py
+++ b/solution.py
@@ -45,6 +45,8 @@
     own_keys,
     new_values,
     attended,
+    raw,
+    weights_v,
     lengths_ref,
     tokens_ref,
     again_ref,
@@ -125,13 +127,14 @@
                 copy.wait()
         for j in range(GROUP):
             s = g * GROUP + j
-            count = lengths_ref[s]
-            q = queries[s]
-            scores = lax.dot_general(
-                q.astype(BF16), kbuf[s], (((1,), (1,)), ((), ())), preferred_element_type=F32
-            ) * scale
-            own = jnp.sum(q * own_keys[pl.ds(s, 1), :], axis=-1, keepdims=True) * scale
-            scores = jnp.where(position < count, scores, -jnp.inf)
+            raw[j] = lax.dot_general(
+                queries[s].astype(BF16), kbuf[s], (((1,), (1,)), ((), ())), preferred_element_type=F32
+            )
+        own_ws = []
+        for j in range(GROUP):
+            s = g * GROUP + j
+            own = jnp.sum(queries[s] * own_keys[pl.ds(s, 1), :], axis=-1, keepdims=True) * scale
+            scores = jnp.where(position < lengths_ref[s], raw[j] * scale, -jnp.inf)
             top = jnp.maximum(jnp.max(scores, axis=-1, keepdims=True), own)
             raised = jnp.exp(scores - top)
             own_raised = jnp.exp(own - top)
@@ -139,15 +142,21 @@
             inv = 1.0 / total
             probs = raised * inv
             own_probs = own_raised * inv
-            mixed = (probs - lam * pltpu.roll(probs, 4, 0)).astype(BF16)
+            weights_v[j] = (probs - lam * pltpu.roll(probs, 4, 0)).astype(BF16)
             own_b = jnp.broadcast_to(own_probs, (8, 128))
-            own_w = (own_b - lam * pltpu.roll(own_b, 4, 0)).astype(BF16).astype(F32)[:, :1]
+            own_ws.append((own_b - lam * pltpu.roll(own_b, 4, 0)).astype(BF16).astype(F32)[:, :1])
+        outs = []
+        for j in range(GROUP):
+            s = g * GROUP + j
+            count = lengths_ref[s]
             pieces = [
                 jnp.where(c * PIECE < count, vbuf[s, c * PIECE:(c + 1) * PIECE, :], jnp.zeros((PIECE, width), BF16))
                 for c in range(length // PIECE)
             ]
-            out = jnp.dot(mixed, jnp.concatenate(pieces, axis=0), preferred_element_type=F32)
-            out = out + own_w * new_values[pl.ds(s, 1), :]
+            outs.append(jnp.dot(weights_v[j], jnp.concatenate(pieces, axis=0), preferred_element_type=F32))
+        for j in range(GROUP):
+            s = g * GROUP + j
+            out = outs[j] + own_ws[j] * new_values[pl.ds(s, 1), :]
             out = jnp.where(mine, out, 0.0)
             mean_sq = jnp.sum(out * out, axis=-1, keepdims=True) * (1.0 / head)
             out = out * lax.rsqrt(mean_sq + EPS)
@@ -175,6 +184,8 @@
         pltpu.VMEM((seqs, width), F32),
         pltpu.VMEM((seqs, width), F32),
         pltpu.VMEM((seqs, width), F32),
+        pltpu.VMEM((GROUP, 8, length), F32),
+        pltpu.VMEM((GROUP, 8, length), BF16),
         pltpu.SMEM((seqs,), jnp.int32),
         pltpu.VMEM(tokens.shape, BF16),
         pltpu.VMEM((1, tokens.shape[1]), F32),
@@ -424,26 +435,28 @@
         mine = hbuf.at[j, t]
         hfar.append(send(mine, mine, hy_s.at[j], hy_r.at[j], (e, across)))
         hnear.append(send(mine, mine, hc_s.at[j], hc_r.at[j], (e, twin)))
-    hrelay = []
-    for j in range(owned):
-        hfar[j].wait_recv()
-        theirs = hbuf.at[j, across]
-        hrelay.append(send(theirs, theirs, hd_s.at[j], hd_r.at[j], (e, twin)))
     deep = hbuf.shape[3]
-    back = []
-    for j in range(owned):
-        hnear[j].wait_recv()
-        hrelay[j].wait_recv()
-        loads[3 * j + 2].wait()
+    hrelay, back = [], []
+    for j in range(owned + 1):
+        if j < owned:
+            hfar[j].wait_recv()
+            theirs = hbuf.at[j, across]
+            hrelay.append(send(theirs, theirs, hd_s.at[j], hd_r.at[j], (e, twin)))
+        if j == 0:
+            continue
+        i = j - 1
+        hnear[i].wait_recv()
+        hrelay[i].wait_recv()
+        loads[3 * i + 2].wait()
         result = jnp.zeros((per, columns), F32)
         for q in range(parts):
-            result += jnp.dot(hbuf[j, q], down_v[j, q * deep:(q + 1) * deep, :], preferred_element_type=F32)
-        resbuf[j] = result.reshape(groups, capacity, columns).astype(BF16)
+            result += jnp.dot(hbuf[i, q], down_v[i, q * deep:(q + 1) * deep, :], preferred_element_type=F32)
+        resbuf[i] = result.reshape(groups, capacity, columns).astype(BF16)
         for k in range(1, groups):
             peer = lax.rem(e + k, groups)
-            i = j * (groups - 1) + k - 1
-            back.append(send(resbuf.at[j, peer], ret.at[e, j], re_s.at[i], re_r.at[i], (peer, t)))
-        ret[e, j] = resbuf[j, e]
+            n_back = i * (groups - 1) + k - 1
+            back.append(send(resbuf.at[i, peer], ret.at[e, i], re_s.at[n_back], re_r.at[n_back], (peer, t)))
+        ret[e, i] = resbuf[i, e]
     for copy in keep + back:
         copy.wait_recv()
     moe = exact_dot(combine_v[...], ret[...].astype(F32).reshape(groups * block, columns))

time: 63.7 us -> 54.6 us (0.86)
  Pallas kernels: 62.3 us -> 53 us
    pallas_call x1, Pallas kernels: 22.6 us -> 14.2 us  [attend(): pl.pallas_call(functools.partial(attend_kernel, heads), out_shape=jax.Sha...]
    pallas_call x1, Pallas kernels: 39.7 us -> 38.8 us  [experts(): pl.pallas_call(functools.partial(experts_kernel, groups, parts, capacity)...]
where the time goes in v1:
time: 54.6 us; the launch traced here: 54.4 us
  Pallas kernels  53 us (97%)
  local copies, waits for them, and re-layouts  1.38 us (3%)
    pallas_call x1, Pallas kernels, experts(): pl.pallas_call(functools.partial(experts_kernel, groups, parts, capacity)...  38.8 us
    pallas_call x1, Pallas kernels, attend(): pl.pallas_call(functools.partial(attend_kernel, heads), out_shape=jax.Sha...  14.2 us
    unnamed x1, local copies, waits for them, and re-layouts  1.38 us

profile of v1, /device:TPU:0, one launch (start us, length us, event | category | flops | bytes accessed | tf_op | source)
XLA Modules:
  0.0 54.4 jit_solution(6538816415775202116)
XLA Ops:
  0.0 14.2 %attend.1.part_ref = bf16[4,8,2048]{2,1,0:T(8,128)(2,1)} custom-call(f32[2]{0:T(128)} %lam_ref.1, s32[32]{0:T(128)} %lengths_hbm.1, bf16[32,2048]{1,0:T(8,128)(2,1)} %tokens_ref.1, f32[1,2048]{1,0:T(1,128)} %bitcast.5, f32[1,128]{1,0:T(1,128)} %bitcast.9, bf16[32,1024,256]{2,1,0:T(8,128)(2,1)} %keys_hbm.1, bf16[32,1024,256]{2,1,0:T(8,128)(2,1)} %values_hbm.1, ...), custom_call_target="tpu_custom_call" | custom-call | tf_op jit(solution)/shard_map/attend/pallas_call | solution.py:198
  14.2 38.8 %experts.1 = bf16[32,512]{1,0:T(8,128)(2,1)} custom-call(bf16[4,8,2048]{2,1,0:T(8,128)(2,1)} %attend.1.part_ref, bf16[32,2048]{1,0:T(8,128)(2,1)} %tokens_ref.1, f32[1,2048]{1,0:T(1,128)} %bitcast.6, s32[4,32]{1,0:T(4,128)} %bitcast.7, f32[4,32]{1,0:T(4,128)} %bitcast.8, bf16[4,2048,256]{2,1,0:T(8,128)(2,1)} %gate_hbm.1, bf16[4,2048,256]{2,1,0:T(8,128)(2,1)} %up_hbm.1, ...), custom_call_target="tpu_custom_call" | custom-call | tf_op jit(solution)/shard_map/experts/pallas_call | solution.py:495
  53.0 1.4 %copy.21 = bf16[32,512]{1,0:T(8,128)(2,1)} copy(bf16[32,512]{1,0:T(8,128)(2,1)} %experts.1) | data formatting | bytes 65536

commit v2 on v1

--- a/solution.py
+++ b/solution.py
@@ -13,6 +13,7 @@
 PIECE = 128
 GROUP = 8
 VMEM_BYTES = 67043328
+LAYER_BYTES = 60 * 1024 * 1024
 F32 = jnp.float32
 BF16 = jnp.bfloat16
 
@@ -261,248 +262,457 @@
     return combine
 
 
-def experts_kernel(
+def flip(index, mask):
+    bit = 1
+    out = index
+    while bit <= mask:
+        if mask & bit:
+            out = out + (1 - 2 * lax.rem(index // bit, 2)) * bit
+        bit *= 2
+    return out
+
+
+def layer_kernel(
+    heads,
     groups,
     parts,
     capacity,
-    part_ref,
-    tokens_ref,
-    fgain_ref,
-    routes_ref,
-    logits_ref,
+    lam_hbm,
+    lengths_hbm,
+    tokens_hbm,
+    again_hbm,
+    hgain_hbm,
+    fgain_hbm,
+    routes_hbm,
+    logits_hbm,
+    keys_hbm,
+    values_hbm,
+    q1_hbm,
+    q2_hbm,
+    k1_hbm,
+    k2_hbm,
+    vw_hbm,
+    ow_hbm,
     gate_hbm,
     up_hbm,
     down_hbm,
     out_ref,
+    kbuf,
+    vbuf,
+    q1_v,
+    q2_v,
+    k1_v,
+    k2_v,
+    vw_v,
+    ow_v,
     gate_v,
     up_v,
     down_v,
+    queries,
+    own_keys,
+    new_values,
+    attended,
+    raw,
+    weights_v,
+    lam_ref,
+    lengths_ref,
+    tokens_ref,
+    again_ref,
+    hgain_ref,
+    fgain_ref,
+    routes_ref,
+    logits_ref,
+    wide_v,
+    part_f,
+    part_b,
     rs_buf,
-    wide,
-    after,
     kept,
     slot_buf,
+    combine_v,
     xbuf,
     hbuf,
     resbuf,
     ret,
-    combine_v,
+    ksem,
+    vsem,
     wsem,
-    rs_s,
+    ssem,
+    snd,
     rs_r,
-    sl_s,
     sl_r,
-    k_s,
-    k_r,
-    xe_s,
-    xe_r,
-    xy_s,
-    xy_r,
-    xc_s,
-    xc_r,
-    xd_s,
-    xd_r,
-    hy_s,
+    ag_r,
+    far_r,
+    near_r,
+    relay_r,
+    tail_r,
     hy_r,
-    hc_s,
     hc_r,
-    hd_s,
     hd_r,
-    re_s,
     re_r,
 ):
     e, t = lax.axis_index("ep"), lax.axis_index("tp")
+    seqs, length, width = kbuf.shape
+    head = width // heads
+    half = head // 2
+    scale = half ** (-0.5)
     owned = gate_v.shape[0]
-    rows, width = after.shape
     columns = out_ref.shape[1]
-    seqs = rows * parts
+    pieces = seqs // GROUP
     top = routes_ref.shape[0]
     n = seqs * top
     block = owned * capacity
+    per = groups * capacity
     twin = t + 1 - 2 * lax.rem(t, 2)
     across = lax.rem(t + 2, parts)
 
-    loads = []
+    smalls = (
+        (lengths_hbm, lengths_ref), (tokens_hbm, tokens_ref), (again_hbm, again_ref), (hgain_hbm, hgain_ref),
+        (fgain_hbm, fgain_ref), (routes_hbm, routes_ref), (logits_hbm, logits_ref), (lam_hbm, lam_ref),
+    )
+    smalls = [pltpu.make_async_copy(src, dst, ssem.at[i]) for i, (src, dst) in enumerate(smalls)]
+    for small in smalls:
+        small.start()
+    weights = [(q1_hbm, q1_v), (q2_hbm, q2_v), (k1_hbm, k1_v), (k2_hbm, k2_v), (vw_hbm, vw_v), (ow_hbm, ow_v)]
     for j in range(owned):
-        for i, (src, dst) in enumerate(((gate_hbm, gate_v), (up_hbm, up_v), (down_hbm, down_v))):
-            loads.append(pltpu.make_async_copy(src.at[j], dst.at[j], wsem.at[3 * j + i]))
-            loads[-1].start()
+        for src, dst in ((gate_hbm, gate_v), (up_hbm, up_v), (down_hbm, down_v)):
+            weights.append((src.at[j], dst.at[j]))
+    loads = [pltpu.make_async_copy(src, dst, wsem.at[i]) for i, (src, dst) in enumerate(weights)]
+    for load in loads[:5]:
+        load.start()
+
+    def arrived(ref, sem):
+        pltpu.make_async_copy(ref, ref, sem).wait()
+
+    def fetch_keys(s):
+        return pltpu.make_async_copy(keys_hbm.at[s], kbuf.at[s], ksem.at[s // GROUP])
+
+    def fetch_values(s):
+        return pltpu.make_async_copy(values_hbm.at[s], vbuf.at[s], vsem.at[s // GROUP])
+
+    def start_all(fetch, g):
+        if g < pieces:
+            for j in range(GROUP):
+                fetch(g * GROUP + j).start()
+
+    start_all(fetch_keys, 0)
 
     barrier = pltpu.get_barrier_semaphore()
     for k in range(1, parts):
         pl.semaphore_signal(barrier, inc=1, device_id=(e, lax.rem(t + k, parts)), device_id_type=MESH)
-    for k in range(1, groups):
-        pl.semaphore_signal(barrier, inc=1, device_id=(lax.rem(e + k, groups), t), device_id_type=MESH)
-    pl.semaphore_wait(barrier, parts + groups - 2)
-
-    sent = []
-
-    def send(src, dst, s_sem, r_sem, device):
-        copy = pltpu.make_async_remote_copy(
+    for m in range(1, groups):
+        pl.semaphore_signal(barrier, inc=1, device_id=(flip(e, m), t), device_id_type=MESH)
+
+    def remote(src, dst, s_sem, r_sem, device):
+        return pltpu.make_async_remote_copy(
             src_ref=src, dst_ref=dst, send_sem=s_sem, recv_sem=r_sem, device_id=device, device_id_type=MESH
         )
+
+    def send(src, dst, s_sem, r_sem, device):
+        copy = remote(src, dst, snd.at[s_sem], r_sem, device)
         copy.start()
-        sent.append(copy)
         return copy
 
-    scatter = []
-    for k in range(1, parts):
-        peer = lax.rem(t + k, parts)
-        scatter.append(send(part_ref.at[peer], rs_buf.at[k - 1], rs_s.at[k - 1], rs_r.at[k - 1], (e, peer)))
-
+    for i in (1, 2):
+        smalls[i].wait()
+    start_all(fetch_values, 0)
+    loads[5].start()
+    start_all(fetch_keys, 1)
+    wide = tokens_ref[...].astype(F32)
+    wide_v[...] = wide
+    own_columns = pl.ds(pl.multiple_of(t * columns, columns), columns)
+    kept[...] = wide_v[:, own_columns].reshape(kept.shape)
+    normed = (
+        wide * lax.rsqrt(jnp.mean(wide * wide, axis=-1, keepdims=True) + EPS) * again_ref[...]
+    ).astype(BF16)
+    for load in loads[:5]:
+        load.wait()
+
+    def project(w):
+        return jnp.dot(normed, w[...], preferred_element_type=F32).astype(BF16).astype(F32)
+
+    q1, q2, k1, k2 = project(q1_v), project(q2_v), project(k1_v), project(k2_v)
+    new_values[...] = project(vw_v)
+    zero = jnp.zeros((seqs, half), F32)
+    queries[...] = jnp.zeros_like(queries)
+    kparts = []
+    for h in range(heads):
+        cut = slice(h * half, (h + 1) * half)
+        kparts += [k1[:, cut], k2[:, cut]]
+        for p, q in ((0, q1), (1, q2)):
+            mixed = [zero] * (2 * heads)
+            mixed[2 * h + p] = q[:, cut]
+            queries[:, 4 * p + h, :] = jnp.concatenate(mixed, axis=-1)
+    own_keys[...] = jnp.concatenate(kparts, axis=-1)
+
+    for i in (0, 3, 4, 5, 6, 7):
+        smalls[i].wait()
+    fgain = fgain_ref[:, own_columns]
+    position = lax.broadcasted_iota(jnp.int32, (8, length), 1)
+    row = lax.broadcasted_iota(jnp.int32, (8, width), 0)
+    mine = row == lax.broadcasted_iota(jnp.int32, (8, width), 1) // head
+    map_row = lax.broadcasted_iota(jnp.int32, (8, 1), 0)
+    lam = jnp.zeros((8, 1), F32)
+    for h in range(heads):
+        lam = jnp.where(map_row == h, lam_ref[h], lam)
+    hgain = jnp.concatenate([hgain_ref[...]] * heads, axis=-1)
+    lane = lax.broadcasted_iota(jnp.int32, (GROUP, 128), 1)
+
+    def attention(g):
+        arrived(kbuf.at[pl.ds(g * GROUP, GROUP)], ksem.at[g])
+        start_all(fetch_values, g + 1)
+        for j in range(GROUP):
+            s = g * GROUP + j
+            raw[j] = lax.dot_general(
+                queries[s].astype(BF16), kbuf[s], (((1,), (1,)), ((), ())), preferred_element_type=F32
+            )
+        own_ws = []
+        for j in range(GROUP):
+            s = g * GROUP + j
+            own = jnp.sum(queries[s] * own_keys[pl.ds(s, 1), :], axis=-1, keepdims=True) * scale
+            scores = jnp.where(position < lengths_ref[s], raw[j] * scale, -jnp.inf)
+            highest = jnp.maximum(jnp.max(scores, axis=-1, keepdims=True), own)
+            raised = jnp.exp(scores - highest)
+            own_raised = jnp.exp(own - highest)
+            total = jnp.sum(raised, axis=-1, keepdims=True) + own_raised
+            inv = 1.0 / total
+            probs = raised * inv
+            own_probs = own_raised * inv
+            weights_v[j] = (probs - lam * pltpu.roll(probs, 4, 0)).astype(BF16)
+            own_b = jnp.broadcast_to(own_probs, (8, 128))
+            own_ws.append((own_b - lam * pltpu.roll(own_b, 4, 0)).astype(BF16).astype(F32)[:, :1])
+        arrived(vbuf.at[pl.ds(g * GROUP, GROUP)], vsem.at[g])
+        start_all(fetch_keys, g + 2)
+        outs = [
+            jnp.dot(weights_v[j], vbuf[g * GROUP + j], preferred_element_type=F32) for j in range(GROUP)
+        ]
+        for j in range(GROUP):
+            s = g * GROUP + j
+            out = outs[j] + own_ws[j] * new_values[pl.ds(s, 1), :]
+            out = jnp.where(mine, out, 0.0)
+            mean_sq = jnp.sum(out * out, axis=-1, keepdims=True) * (1.0 / head)
+            out = out * lax.rsqrt(mean_sq + EPS)
+            attended[pl.ds(s, 1), :] = jnp.sum(out, axis=0, keepdims=True) * hgain
+
+    def send_partials(g):
+        heads_out = attended[g * GROUP:(g + 1) * GROUP, :].astype(BF16)
+        partial = jnp.dot(heads_out, ow_v[...], preferred_element_type=F32)
+        for q in range(parts):
+            cut = partial[:, q * columns:(q + 1) * columns]
+            part_f[q] = cut
+            part_b[g, q] = cut.astype(BF16)
+        for k in range(1, parts):
+            peer = lax.rem(t + k, parts)
+            send(part_b.at[g, peer], rs_buf.at[g, k - 1], 0, rs_r.at[g], (e, peer))
+        kept[g] = kept[g] + part_f[t]
+
+    gather, far, tail = {}, {}, {}
+    opposite = lax.rem(twin + 2, parts)
+    last = pieces - 1
+
+    def late(g, m):
+        return g == last and m >= groups // 2
+
+    def forward(g, m):
+        view = xbuf.at[g, t, flip(e, m)]
+        far[g, m] = send(view, view, 3, far_r.at[g, m], (e, across))
+        if late(g, m):
+            tail[m] = send(view, view, 3, tail_r.at[m], (e, opposite))
+        send(view, view, 3, near_r.at[0], (e, twin))
+
+    def relay_rows(g):
+        for m in range(groups):
+            far[g, m].wait_recv()
+            if not late(g, m):
+                view = xbuf.at[g, across, flip(e, m)]
+                send(view, view, 3, relay_r.at[int(g == last)], (e, twin))
+
+    def send_rows(g):
+        arrived(rs_buf.at[g], rs_r.at[g])
+        total = kept[g]
+        for k in range(1, parts):
+            total = total + rs_buf[g, k - 1].astype(F32)
+        kept[g] = total
+        squares = jnp.sum(total * total, axis=-1, keepdims=True)
+        high = jnp.broadcast_to(squares, (GROUP, 128)).astype(BF16)
+        low = jnp.broadcast_to(squares, (GROUP, 128)) - high.astype(F32)
+        xbuf[g, t, e, :, :columns] = (total * fgain).astype(BF16)
+        xbuf[g, t, e, :, columns:] = jnp.where(lane < 64, high.astype(F32), low).astype(BF16)
+        view = xbuf.at[g, t, e]
+        for m in range(groups - 1, 0, -1):
+            gather[g, m] = send(view, view, 2, ag_r.at[g, m - 1], (flip(e, m), t))
+        forward(g, 0)
+
+    def forward_rows(g):
+        for m in range(1, groups):
+            gather[g, m].wait_recv()
+            forward(g, m)
+
+    for g in range(pieces):
+        attention(g)
+        if g == 0:
+            pl.semaphore_wait(barrier, parts + groups - 2)
+            loads[5].wait()
+        send_partials(g)
+        if g >= 1:
+            send_rows(g - 1)
+        if g >= 2:
+            forward_rows(g - 2)
+        if g >= 3:
+            relay_rows(g - 3)
+
+    fetches = loads[6:]
+    third = owned
+    for load in fetches[:third]:
+        load.start()
     slot_row, later = route_tables(routes_ref[...], logits_ref[...], groups * block, capacity)
     slot_buf[e] = jnp.broadcast_to(slot_row, (8, n))
-    tables = []
-    for k in range(1, groups):
-        tables.append(
-            send(slot_buf.at[e], slot_buf.at[e], sl_s.at[k - 1], sl_r.at[k - 1], (lax.rem(e + k, groups), t))
-        )
-    wide[...] = tokens_ref[...].astype(F32).reshape(parts, rows, width)
-    total = part_ref[t].astype(F32)
-    for k in range(1, parts):
-        scatter[k - 1].wait_recv()
-        total = total + rs_buf[k - 1].astype(F32)
-    total = wide[t] + total
-    after[...] = total
-    xbuf[e, t] = rms_scale(total, fgain_ref[...]).astype(BF16)
-
-    inner = 2 if groups % 2 == 0 else 1
-    outer = groups // inner
-    place_out, place_in = e // inner, lax.rem(e, inner)
-    gather = []
-    for m in range(1, outer):
-        peer = lax.rem(place_out + m, outer) * inner + place_in
-        gather.append(send(xbuf.at[e, t], xbuf.at[e, t], xe_s.at[m - 1], xe_r.at[m - 1], (peer, t)))
-    side = place_out * inner + inner - 1 - place_in
-    turns = [(0, 0)]
-    for m in range(1, outer):
-        turns += [(m, 0)] + [(m - 1, 1)] * (inner - 1)
-    turns += [(outer - 1, 1)] * (inner - 1)
-    passed = [None] * outer
-    sources = []
-    far, near, relay = [], [], []
-    for k, (m, other) in enumerate(turns):
-        line_in = inner - 1 - place_in if other else place_in
-        source = lax.rem(place_out - m + outer, outer) * inner + line_in
-        sources.append(source)
-        if other:
-            passed[m].wait_recv()
-        elif m:
-            gather[m - 1].wait_recv()
-        if inner > 1 and not other:
-            i = outer - 1 + m
-            passed[m] = send(xbuf.at[source, t], xbuf.at[source, t], xe_s.at[i], xe_r.at[i], (side, t))
-        mine = xbuf.at[source, t]
-        far.append(send(mine, mine, xy_s.at[k], xy_r.at[k], (e, across)))
-        near.append(send(mine, mine, xc_s.at[k], xc_r.at[k], (e, twin)))
-        if k == 0:
-            combine_v[...] = later()
-            keep = []
-            kept[t] = after[:, pl.ds(pl.multiple_of(t * columns, columns), columns)]
-            for q in range(1, parts):
-                peer = lax.rem(t + q, parts)
-                view = after.at[:, pl.ds(pl.multiple_of(peer * columns, columns), columns)]
-                keep.append(send(view, kept.at[t], k_s.at[q - 1], k_r.at[q - 1], (e, peer)))
-    for table in tables:
-        table.wait_recv()
+    for m in range(groups - 1, 0, -1):
+        send(slot_buf.at[e], slot_buf.at[e], 1, sl_r.at[0], (flip(e, m), t))
+    combine_v[...] = later()
+    send_rows(last)
+    for load in fetches[third:]:
+        load.start()
+    for g in range(max(pieces - 3, 0), pieces - 2):
+        relay_rows(g)
+    forward_rows(pieces - 2)
+    forward_rows(last)
+    arrived(slot_buf.at[pl.ds(0, groups - 1)], sl_r.at[0])
     base = e * block
     local = (where_is((block, n), 0) + base).astype(F32)
+    tokens_all = groups * seqs
+    token = where_is((n, tokens_all), 0) // top
+    spot_row = token // GROUP * (groups * GROUP) + token % GROUP
     place = []
     for b in range(groups):
         chosen = (slot_buf[b][:1, :] == local).astype(BF16)
-        spot = (where_is((n, groups * seqs), 1) == where_is((n, groups * seqs), 0) // top + b * seqs).astype(BF16)
+        spot = (where_is((n, tokens_all), 1) == spot_row + b * GROUP).astype(BF16)
         placed = jnp.dot(chosen, spot, preferred_element_type=F32)
-        place.append(placed.reshape(owned, 1, capacity, groups * seqs))
-    dispatch = jnp.concatenate(place, axis=1).reshape(groups * block, groups * seqs).astype(BF16)
-    for k, source in enumerate(sources):
-        far[k].wait_recv()
-        theirs = xbuf.at[source, across]
-        relay.append(send(theirs, theirs, xd_s.at[k], xd_r.at[k], (e, twin)))
-    for copy in near + relay:
+        place.append(placed.reshape(owned, 1, capacity, tokens_all))
+    dispatch = jnp.concatenate(place, axis=1).reshape(groups * block, tokens_all).astype(BF16)
+
+    relay_rows(pieces - 2)
+    relay_rows(last)
+    arrived(xbuf.at[:, 0], near_r.at[0])
+    arrived(xbuf.at[pl.ds(0, last), 0], relay_r.at[0])
+    arrived(xbuf.at[last, 0, pl.ds(0, groups // 2)], relay_r.at[1])
+    for copy in tail.values():
         copy.wait_recv()
 
-    everything = xbuf[...].astype(F32).reshape(groups * seqs, width).astype(BF16)
-    lines = jnp.dot(dispatch, everything, preferred_element_type=F32).astype(BF16)
-    per = groups * capacity
+    lines, squares = [], jnp.zeros((groups * block, 128), F32)
+    for q in range(parts):
+        rows = xbuf[:, q].astype(F32).reshape(tokens_all, columns + 128).astype(BF16)
+        picked = jnp.dot(dispatch, rows, preferred_element_type=F32)
+        lines.append(picked[:, :columns].astype(BF16))
+        squares = squares + picked[:, columns:]
+    lines = jnp.concatenate(lines, axis=-1)
+    mean_sq = (squares[:, :1] + squares[:, 64:65]) * (1.0 / (columns * parts))
+    row_scale = lax.rsqrt(mean_sq + EPS)
     hfar, hnear = [], []
     for j in range(owned):
         for i in range(2):
-            loads[3 * j + i].wait()
+            loads[6 + 3 * j + i].wait()
         line = lines[j * per:(j + 1) * per]
-        gate = jnp.minimum(jnp.dot(line, gate_v[j], preferred_element_type=F32), LIMIT)
-        up = jnp.clip(jnp.dot(line, up_v[j], preferred_element_type=F32), -LIMIT, LIMIT)
+        line_scale = row_scale[j * per:(j + 1) * per]
+        gate = jnp.minimum(jnp.dot(line, gate_v[j], preferred_element_type=F32) * line_scale, LIMIT)
+        up = jnp.clip(jnp.dot(line, up_v[j], preferred_element_type=F32) * line_scale, -LIMIT, LIMIT)
         hbuf[j, t] = ((up + 1.0) * gate * jax.nn.sigmoid(ALPHA * gate)).astype(BF16)
-        mine = hbuf.at[j, t]
-        hfar.append(send(mine, mine, hy_s.at[j], hy_r.at[j], (e, across)))
-        hnear.append(send(mine, mine, hc_s.at[j], hc_r.at[j], (e, twin)))
+        view = hbuf.at[j, t]
+        hfar.append(send(view, view, 4, hy_r.at[j], (e, across)))
+        if j == 0:
+            hrelay = [send(view, view, 4, hd_r.at[j], (e, opposite))]
+        hnear.append(send(view, view, 4, hc_r.at[j], (e, twin)))
     deep = hbuf.shape[3]
-    hrelay, back = [], []
     for j in range(owned + 1):
         if j < owned:
             hfar[j].wait_recv()
             theirs = hbuf.at[j, across]
-            hrelay.append(send(theirs, theirs, hd_s.at[j], hd_r.at[j], (e, twin)))
+            if j:
+                hrelay.append(send(theirs, theirs, 4, hd_r.at[j], (e, twin)))
         if j == 0:
             continue
         i = j - 1
         hnear[i].wait_recv()
         hrelay[i].wait_recv()
-        loads[3 * i + 2].wait()
+        loads[6 + 3 * i + 2].wait()
         result = jnp.zeros((per, columns), F32)
         for q in range(parts):
             result += jnp.dot(hbuf[i, q], down_v[i, q * deep:(q + 1) * deep, :], preferred_element_type=F32)
         resbuf[i] = result.reshape(groups, capacity, columns).astype(BF16)
-        for k in range(1, groups):
-            peer = lax.rem(e + k, groups)
-            n_back = i * (groups - 1) + k - 1
-            back.append(send(resbuf.at[i, peer], ret.at[e, i], re_s.at[n_back], re_r.at[n_back], (peer, t)))
+        for m in range(groups - 1, 0, -1):
+            peer = flip(e, m)
+            send(resbuf.at[i, peer], ret.at[e, i], 5, re_r.at[0], (peer, t))
         ret[e, i] = resbuf[i, e]
-    for copy in keep + back:
-        copy.wait_recv()
+    arrived(ret.at[pl.ds(0, groups - 1)], re_r.at[0])
     moe = exact_dot(combine_v[...], ret[...].astype(F32).reshape(groups * block, columns))
     out_ref[...] = (kept[...].reshape(seqs, columns) + moe).astype(out_ref.dtype)
-    for copy in sent:
-        copy.wait_send()
-
-
-def experts(part, tokens, ffn_gain, routes, logits, gate_w, up_w, down_w, groups, parts, capacity):
-    seqs, width = tokens.shape
-    rows = seqs // parts
+    arrived(part_b.at[:, pl.ds(0, parts - 1)], snd.at[0])
+    arrived(slot_buf.at[pl.ds(0, groups - 1)], snd.at[1])
+    arrived(xbuf.at[:, 0, pl.ds(0, groups - 1)], snd.at[2])
+    arrived(xbuf.at[:, pl.ds(0, parts - 1)], snd.at[3])
+    arrived(hbuf.at[:, pl.ds(0, parts - 1)], snd.at[4])
+    arrived(resbuf.at[:, pl.ds(0, groups - 1)], snd.at[5])
+
+
+def layer(
+    tokens, lengths, cache_keys, cache_values, attn_gain, q1w, q2w, k1w, k2w, vw, lam, hgain, out_w,
+    ffn_gain, routes, logits, gate_w, up_w, down_w, groups, parts, capacity,
+):
+    seqs, length, width = cache_keys.shape
+    heads = lam.shape[0]
     owned, _, deep = gate_w.shape
     columns = down_w.shape[2]
     per = groups * capacity
-    vm = pl.BlockSpec(memory_space=pltpu.VMEM)
+    pieces = seqs // GROUP
+    full = tokens.shape[1]
+    routes, logits = routes.T, logits.T
     anyspace = pl.BlockSpec(memory_space=pltpu.HBM)
-    dma = lambda count: [pltpu.SemaphoreType.DMA((count,)), pltpu.SemaphoreType.DMA((count,))]
-    scratch = [
-        pltpu.VMEM(gate_w.shape, BF16),
-        pltpu.VMEM(up_w.shape, BF16),
-        pltpu.VMEM(down_w.shape, BF16),
-        pltpu.VMEM((parts - 1, rows, width), BF16),
-        pltpu.VMEM((parts, rows, width), F32),
-        pltpu.VMEM((rows, width), F32),
-        pltpu.VMEM((parts, rows, columns), F32),
+    scratch = [pltpu.VMEM(cache_keys.shape, BF16), pltpu.VMEM(cache_values.shape, BF16)]
+    scratch += [pltpu.VMEM(w.shape, BF16) for w in (q1w, q2w, k1w, k2w, vw, out_w, gate_w, up_w, down_w)]
+    scratch += [
+        pltpu.VMEM((seqs, 8, width), F32),
+        pltpu.VMEM((seqs, width), F32),
+        pltpu.VMEM((seqs, width), F32),
+        pltpu.VMEM((seqs, width), F32),
+        pltpu.VMEM((GROUP, 8, length), F32),
+        pltpu.VMEM((GROUP, 8, length), BF16),
+        pltpu.SMEM(lam.shape, F32),
+        pltpu.SMEM((seqs,), jnp.int32),
+        pltpu.VMEM(tokens.shape, BF16),
+        pltpu.VMEM((1, full), F32),
+        pltpu.VMEM((1, hgain.shape[0]), F32),
+        pltpu.VMEM((1, full), F32),
+        pltpu.VMEM(routes.shape, routes.dtype),
+        pltpu.VMEM(logits.shape, F32),
+        pltpu.VMEM(tokens.shape, F32),
+        pltpu.VMEM((parts, GROUP, columns), F32),
+        pltpu.VMEM((pieces, parts, GROUP, columns), BF16),
+        pltpu.VMEM((pieces, parts - 1, GROUP, columns), BF16),
+        pltpu.VMEM((pieces, GROUP, columns), F32),
         pltpu.VMEM((groups, 8, routes.size), F32),
-        pltpu.VMEM((groups, parts, rows, width), BF16),
+        pltpu.VMEM((seqs, owned * per), F32),
+        pltpu.VMEM((pieces, parts, groups, GROUP, columns + 128), BF16),
         pltpu.VMEM((owned, parts, per, deep), BF16),
         pltpu.VMEM((owned, groups, capacity, columns), BF16),
         pltpu.VMEM((groups, owned, capacity, columns), BF16),
-        pltpu.VMEM((seqs, owned * per), F32),
-        pltpu.SemaphoreType.DMA((3 * owned,)),
     ]
-    scratch += dma(parts - 1) + dma(groups - 1) + dma(parts - 1) + dma(groups - 1)
-    scratch += dma(groups) * 3 + dma(owned) * 3 + dma(owned * (groups - 1))
+    dma = lambda *shape: [pltpu.SemaphoreType.DMA(shape)]
+    scratch += dma(pieces) * 2 + dma(6 + 3 * owned) + dma(8)
+    scratch += dma(6) + dma(pieces) + dma(1) + dma(pieces, groups - 1)
+    scratch += dma(pieces, groups) + dma(1) + dma(2) + dma(groups) + dma(owned) * 3 + dma(1)
     return pl.pallas_call(
-        functools.partial(experts_kernel, groups, parts, capacity),
+        functools.partial(layer_kernel, heads, groups, parts, capacity),
         out_shape=jax.ShapeDtypeStruct((seqs, columns), BF16),
-        in_specs=[vm] * 5 + [anyspace] * 3,
-        out_specs=vm,
+        in_specs=[anyspace] * 19,
+        out_specs=pl.BlockSpec(memory_space=pltpu.VMEM),
         scratch_shapes=scratch,
         compiler_params=pltpu.CompilerParams(
-            collective_id=0, has_side_effects=True, vmem_limit_bytes=VMEM_BYTES
+            collective_id=0, has_side_effects=True, vmem_limit_bytes=LAYER_BYTES
         ),
-        name="experts",
-    )(part, tokens, ffn_gain.reshape(1, -1), routes.T, logits.T, gate_w, up_w, down_w)
+        name="layer",
+    )(
+        lam, lengths, tokens, attn_gain.reshape(1, -1), hgain.reshape(1, -1), ffn_gain.reshape(1, -1),
+        routes, logits, cache_keys, cache_values, q1w, q2w, k1w, k2w, vw, out_w, gate_w, up_w, down_w,
+    )
 
 
 def slot_tables(routes, weights, expert_ids, capacity):
@@ -562,7 +772,15 @@
     owned = gate_w.shape[0]
     seqs, top = routes.shape
     capacity = max(2, 2 * seqs * top // (owned * groups))
-    fused = parts == 4 and seqs % (8 * parts) == 0 and capacity % 8 == 0 and seqs * top % 128 == 0
+    fused = (
+        parts == 4 and seqs % GROUP == 0 and capacity % 8 == 0 and seqs * top % 128 == 0 and groups & (groups - 1) == 0
+    )
+    if fused:
+        return layer(
+            tokens, lengths, cache_keys, cache_values, attn_gain, q_first_w, q_second_w, k_first_w, k_second_w,
+            value_w, mix_lambda, head_gain, out_w, ffn_gain, routes, route_logits, gate_w, up_w, down_w,
+            groups, parts, capacity,
+        )
     partial_value = attend(
         tokens,
         lengths,
@@ -577,13 +795,9 @@
         mix_lambda,
         head_gain,
         out_w,
-        BF16 if fused else F32,
-        parts if fused else 1,
-    )
-    if fused:
-        return experts(
-            partial_value, tokens, ffn_gain, routes, route_logits, gate_w, up_w, down_w, groups, parts, capacity
-        )
+        F32,
+        1,
+    )
     partial_value = partial_value.reshape(tokens.shape)
     wide = tokens.astype(F32)
     columns = wide.shape[1] // lax.axis_size("tp")

time: 54.6 us -> 47.5 us (0.87)
  Pallas kernels: 53 us -> 46 us
    pallas_call x2 -> x1, Pallas kernels: 53 us -> 46 us  [layer(): pl.pallas_call(functools.partial(layer_kernel, heads, groups, parts, capa...]
where the time goes in v2:
time: 47.5 us; the launch traced here: 47.4 us
  Pallas kernels  46 us (97%)
  local copies, waits for them, and re-layouts  1.38 us (3%)
    pallas_call x1, Pallas kernels, layer(): pl.pallas_call(functools.partial(layer_kernel, heads, groups, parts, capa...  46 us
    unnamed x1, local copies, waits for them, and re-layouts  1.38 us

profile of v2, /device:TPU:0, one launch (start us, length us, event | category | flops | bytes accessed | tf_op | source)
XLA Modules:
  0.0 47.4 jit_solution(14994816293488132971)
XLA Ops:
  0.0 46.0 %layer.1 = bf16[32,512]{1,0:T(8,128)(2,1)} custom-call(f32[2]{0:T(128)} %lam_hbm.1, s32[32]{0:T(128)} %lengths_hbm.1, bf16[32,2048]{1,0:T(8,128)(2,1)} %tokens_hbm.1, f32[1,2048]{1,0:T(1,128)} %bitcast.5, f32[1,128]{1,0:T(1,128)} %bitcast.9, f32[1,2048]{1,0:T(1,128)} %bitcast.6, s32[4,32]{1,0:T(4,128)} %bitcast.7, f32[4,32]{1,0:T(4,128)} %bitcast.8, ...), custom_call_target="tpu_custom_call" | custom-call | tf_op jit(solution)/shard_map/layer/pallas_call | solution.py:702
  46.0 1.4 %copy.21 = bf16[32,512]{1,0:T(8,128)(2,1)} copy(bf16[32,512]{1,0:T(8,128)(2,1)} %layer.1) | data formatting | bytes 65536

commit v3 on v2

--- a/solution.py
+++ b/solution.py
@@ -394,7 +394,8 @@
             for j in range(GROUP):
                 fetch(g * GROUP + j).start()
 
-    start_all(fetch_keys, 0)
+    for j in range(GROUP // 2):
+        fetch_keys(j).start()
 
     barrier = pltpu.get_barrier_semaphore()
     for k in range(1, parts):
@@ -414,9 +415,10 @@
 
     for i in (1, 2):
         smalls[i].wait()
+    for j in range(GROUP // 2, GROUP):
+        fetch_keys(j).start()
     start_all(fetch_values, 0)
     loads[5].start()
-    start_all(fetch_keys, 1)
     wide = tokens_ref[...].astype(F32)
     wide_v[...] = wide
     own_columns = pl.ds(pl.multiple_of(t * columns, columns), columns)
@@ -426,6 +428,7 @@
     ).astype(BF16)
     for load in loads[:5]:
         load.wait()
+    start_all(fetch_keys, 1)
 
     def project(w):
         return jnp.dot(normed, w[...], preferred_element_type=F32).astype(BF16).astype(F32)
@@ -455,7 +458,6 @@
     for h in range(heads):
         lam = jnp.where(map_row == h, lam_ref[h], lam)
     hgain = jnp.concatenate([hgain_ref[...]] * heads, axis=-1)
-    lane = lax.broadcasted_iota(jnp.int32, (GROUP, 128), 1)
 
     def attention(g):
         arrived(kbuf.at[pl.ds(g * GROUP, GROUP)], ksem.at[g])
@@ -532,20 +534,18 @@
         for k in range(1, parts):
             total = total + rs_buf[g, k - 1].astype(F32)
         kept[g] = total
-        squares = jnp.sum(total * total, axis=-1, keepdims=True)
-        high = jnp.broadcast_to(squares, (GROUP, 128)).astype(BF16)
-        low = jnp.broadcast_to(squares, (GROUP, 128)) - high.astype(F32)
-        xbuf[g, t, e, :, :columns] = (total * fgain).astype(BF16)
-        xbuf[g, t, e, :, columns:] = jnp.where(lane < 64, high.astype(F32), low).astype(BF16)
+        xbuf[g, t, e] = (total * fgain).astype(BF16)
         view = xbuf.at[g, t, e]
         for m in range(groups - 1, 0, -1):
             gather[g, m] = send(view, view, 2, ag_r.at[g, m - 1], (flip(e, m), t))
         forward(g, 0)
 
-    def forward_rows(g):
-        for m in range(1, groups):
+    def forward_rows(g, sources):
+        for m in sources:
             gather[g, m].wait_recv()
             forward(g, m)
+
+    close, distant = range(1, groups // 2), range(groups // 2, groups)
 
     for g in range(pieces):
         attention(g)
@@ -555,10 +555,10 @@
         send_partials(g)
         if g >= 1:
             send_rows(g - 1)
+        if g >= 3:
+            forward_rows(g - 3, distant)
         if g >= 2:
-            forward_rows(g - 2)
-        if g >= 3:
-            relay_rows(g - 3)
+            forward_rows(g - 2, close)
 
     fetches = loads[6:]
     third = owned
@@ -568,14 +568,21 @@
     slot_buf[e] = jnp.broadcast_to(slot_row, (8, n))
     for m in range(groups - 1, 0, -1):
         send(slot_buf.at[e], slot_buf.at[e], 1, sl_r.at[0], (flip(e, m), t))
-    combine_v[...] = later()
+    share = later()
+    for i in range(3):
+        coarse = share.astype(BF16)
+        combine_v[i * seqs:(i + 1) * seqs, :] = coarse
+        share = share - coarse.astype(F32)
+    forward_rows(last - 2, distant)
     send_rows(last)
     for load in fetches[third:]:
         load.start()
-    for g in range(max(pieces - 3, 0), pieces - 2):
+    for g in range(last - 1):
         relay_rows(g)
-    forward_rows(pieces - 2)
-    forward_rows(last)
+    forward_rows(last - 1, close)
+    forward_rows(last - 1, distant)
+    forward_rows(last, close)
+    forward_rows(last, distant)
     arrived(slot_buf.at[pl.ds(0, groups - 1)], sl_r.at[0])
     base = e * block
     local = (where_is((block, n), 0) + base).astype(F32)
@@ -590,7 +597,7 @@
         place.append(placed.reshape(owned, 1, capacity, tokens_all))
     dispatch = jnp.concatenate(place, axis=1).reshape(groups * block, tokens_all).astype(BF16)
 
-    relay_rows(pieces - 2)
+    relay_rows(last - 1)
     relay_rows(last)
     arrived(xbuf.at[:, 0], near_r.at[0])
     arrived(xbuf.at[pl.ds(0, last), 0], relay_r.at[0])
@@ -598,14 +605,15 @@
     for copy in tail.values():
         copy.wait_recv()
 
-    lines, squares = [], jnp.zeros((groups * block, 128), F32)
+    lines, squares = [], jnp.zeros((groups * block, columns), F32)
     for q in range(parts):
-        rows = xbuf[:, q].astype(F32).reshape(tokens_all, columns + 128).astype(BF16)
+        rows = xbuf[:, q].astype(F32).reshape(tokens_all, columns).astype(BF16)
         picked = jnp.dot(dispatch, rows, preferred_element_type=F32)
-        lines.append(picked[:, :columns].astype(BF16))
-        squares = squares + picked[:, columns:]
+        lines.append(picked.astype(BF16))
+        plain = picked * (1.0 / fgain_ref[:, q * columns:(q + 1) * columns])
+        squares = squares + plain * plain
     lines = jnp.concatenate(lines, axis=-1)
-    mean_sq = (squares[:, :1] + squares[:, 64:65]) * (1.0 / (columns * parts))
+    mean_sq = jnp.sum(squares, axis=-1, keepdims=True) * (1.0 / (columns * parts))
     row_scale = lax.rsqrt(mean_sq + EPS)
     hfar, hnear = [], []
     for j in range(owned):
@@ -643,7 +651,9 @@
             send(resbuf.at[i, peer], ret.at[e, i], 5, re_r.at[0], (peer, t))
         ret[e, i] = resbuf[i, e]
     arrived(ret.at[pl.ds(0, groups - 1)], re_r.at[0])
-    moe = exact_dot(combine_v[...], ret[...].astype(F32).reshape(groups * block, columns))
+    results = ret[...].astype(F32).reshape(groups * block, columns).astype(BF16)
+    moe = jnp.dot(combine_v[...], results, preferred_element_type=F32)
+    moe = moe[:seqs] + moe[seqs:2 * seqs] + moe[2 * seqs:]
     out_ref[...] = (kept[...].reshape(seqs, columns) + moe).astype(out_ref.dtype)
     arrived(part_b.at[:, pl.ds(0, parts - 1)], snd.at[0])
     arrived(slot_buf.at[pl.ds(0, groups - 1)], snd.at[1])
@@ -689,8 +699,8 @@
         pltpu.VMEM((pieces, parts - 1, GROUP, columns), BF16),
         pltpu.VMEM((pieces, GROUP, columns), F32),
         pltpu.VMEM((groups, 8, routes.size), F32),
-        pltpu.VMEM((seqs, owned * per), F32),
-        pltpu.VMEM((pieces, parts, groups, GROUP, columns + 128), BF16),
+        pltpu.VMEM((3 * seqs, owned * per), BF16),
+        pltpu.VMEM((pieces, parts, groups, GROUP, columns), BF16),
         pltpu.VMEM((owned, parts, per, deep), BF16),
         pltpu.VMEM((owned, groups, capacity, columns), BF16),
         pltpu.VMEM((groups, owned, capacity, columns), BF16),
@@ -701,7 +711,7 @@
     scratch += dma(pieces, groups) + dma(1) + dma(2) + dma(groups) + dma(owned) * 3 + dma(1)
     return pl.pallas_call(
         functools.partial(layer_kernel, heads, groups, parts, capacity),
-        out_shape=jax.ShapeDtypeStruct((seqs, columns), BF16),
+        out_shape=pltpu.VMEM((seqs, columns), BF16),
         in_specs=[anyspace] * 19,
         out_specs=pl.BlockSpec(memory_space=pltpu.VMEM),
         scratch_shapes=scratch,
@@ -773,7 +783,7 @@
     seqs, top = routes.shape
     capacity = max(2, 2 * seqs * top // (owned * groups))
     fused = (
-        parts == 4 and seqs % GROUP == 0 and capacity % 8 == 0 and seqs * top % 128 == 0 and groups & (groups - 1) == 0
+        parts == 4 and seqs % GROUP == 0 and seqs >= 4 * GROUP and capacity % 8 == 0 and seqs * top % 128 == 0 and groups & (groups - 1) == 0
     )
     if fused:
         return layer(

time: 47.5 us -> 44.7 us (0.941)
  Pallas kernels: 46 us -> 43.9 us
  local copies, waits for them, and re-layouts: 1.38 us -> 0.62 us
    pallas_call x1, Pallas kernels: 46 us -> 43.9 us  [layer(): pl.pallas_call(functools.partial(layer_kernel, heads, groups, parts, capa...]
    unnamed x1, local copies, waits for them, and re-layouts: 1.38 us -> 0.62 us
where the time goes in v3:
time: 44.7 us; the launch traced here: 44.6 us
  Pallas kernels  43.9 us (98%)
  local copies, waits for them, and re-layouts  0.62 us (1%)
    pallas_call x1, Pallas kernels, layer(): pl.pallas_call(functools.partial(layer_kernel, heads, groups, parts, capa...  43.9 us

profile of v3, /device:TPU:0, one launch (start us, length us, event | category | flops | bytes accessed | tf_op | source)
XLA Modules:
  0.0 44.6 jit_solution(3727170717106987728)
XLA Ops:
  0.0 43.9 %layer.1 = bf16[32,512]{1,0:T(8,128)(2,1)S(1)} custom-call(f32[2]{0:T(128)} %lam_hbm.1, s32[32]{0:T(128)} %lengths_hbm.1, bf16[32,2048]{1,0:T(8,128)(2,1)} %tokens_hbm.1, f32[1,2048]{1,0:T(1,128)} %bitcast.5, f32[1,128]{1,0:T(1,128)} %bitcast.9, f32[1,2048]{1,0:T(1,128)} %bitcast.6, s32[4,32]{1,0:T(4,128)} %bitcast.7, f32[4,32]{1,0:T(4,128)} %bitcast.8, ...), custom_call_target="tpu_custom_call" | custom-call | tf_op jit(solution)/shard_map/layer/pallas_call | solution.py:712
  44.0 0.6 %copy.21 = bf16[32,512]{1,0:T(8,128)(2,1)} copy(bf16[32,512]{1,0:T(8,128)(2,1)S(1)} %layer.1) | data formatting | bytes 65536

commit v4 on v3

--- a/solution.py
+++ b/solution.py
@@ -329,6 +329,8 @@
     kept,
     slot_buf,
     combine_v,
+    dispatch_v,
+    lines_v,
     xbuf,
     hbuf,
     resbuf,
@@ -340,11 +342,9 @@
     snd,
     rs_r,
     sl_r,
-    ag_r,
-    far_r,
-    near_r,
-    relay_r,
-    tail_r,
+    own_r,
+    wide_r,
+    join_r,
     hy_r,
     hc_r,
     hd_r,
@@ -401,7 +401,8 @@
     for k in range(1, parts):
         pl.semaphore_signal(barrier, inc=1, device_id=(e, lax.rem(t + k, parts)), device_id_type=MESH)
     for m in range(1, groups):
-        pl.semaphore_signal(barrier, inc=1, device_id=(flip(e, m), t), device_id_type=MESH)
+        for side in (t, across):
+            pl.semaphore_signal(barrier, inc=1, device_id=(flip(e, m), side), device_id_type=MESH)
 
     def remote(src, dst, s_sem, r_sem, device):
         return pltpu.make_async_remote_copy(
@@ -417,8 +418,6 @@
         smalls[i].wait()
     for j in range(GROUP // 2, GROUP):
         fetch_keys(j).start()
-    start_all(fetch_values, 0)
-    loads[5].start()
     wide = tokens_ref[...].astype(F32)
     wide_v[...] = wide
     own_columns = pl.ds(pl.multiple_of(t * columns, columns), columns)
@@ -426,8 +425,19 @@
     normed = (
         wide * lax.rsqrt(jnp.mean(wide * wide, axis=-1, keepdims=True) + EPS) * again_ref[...]
     ).astype(BF16)
+    for i in (4, 5, 6):
+        smalls[i].wait()
+    slot_row, later = route_tables(routes_ref[...], logits_ref[...], groups * block, capacity)
+    slot_buf[e] = jnp.broadcast_to(slot_row, (8, n))
+    share = later()
+    for i in range(3):
+        coarse = share.astype(BF16)
+        combine_v[i * seqs:(i + 1) * seqs, :] = coarse
+        share = share - coarse.astype(F32)
     for load in loads[:5]:
         load.wait()
+    start_all(fetch_values, 0)
+    loads[5].start()
     start_all(fetch_keys, 1)
 
     def project(w):
@@ -447,7 +457,7 @@
             queries[:, 4 * p + h, :] = jnp.concatenate(mixed, axis=-1)
     own_keys[...] = jnp.concatenate(kparts, axis=-1)
 
-    for i in (0, 3, 4, 5, 6, 7):
+    for i in (0, 3, 7):
         smalls[i].wait()
     fgain = fgain_ref[:, own_columns]
     position = lax.broadcasted_iota(jnp.int32, (8, length), 1)
@@ -507,26 +517,8 @@
             send(part_b.at[g, peer], rs_buf.at[g, k - 1], 0, rs_r.at[g], (e, peer))
         kept[g] = kept[g] + part_f[t]
 
-    gather, far, tail = {}, {}, {}
+    own, last = {}, pieces - 1
     opposite = lax.rem(twin + 2, parts)
-    last = pieces - 1
-
-    def late(g, m):
-        return g == last and m >= groups // 2
-
-    def forward(g, m):
-        view = xbuf.at[g, t, flip(e, m)]
-        far[g, m] = send(view, view, 3, far_r.at[g, m], (e, across))
-        if late(g, m):
-            tail[m] = send(view, view, 3, tail_r.at[m], (e, opposite))
-        send(view, view, 3, near_r.at[0], (e, twin))
-
-    def relay_rows(g):
-        for m in range(groups):
-            far[g, m].wait_recv()
-            if not late(g, m):
-                view = xbuf.at[g, across, flip(e, m)]
-                send(view, view, 3, relay_r.at[int(g == last)], (e, twin))
 
     def send_rows(g):
         arrived(rs_buf.at[g], rs_r.at[g])
@@ -537,106 +529,121 @@
         xbuf[g, t, e] = (total * fgain).astype(BF16)
         view = xbuf.at[g, t, e]
         for m in range(groups - 1, 0, -1):
-            gather[g, m] = send(view, view, 2, ag_r.at[g, m - 1], (flip(e, m), t))
-        forward(g, 0)
-
-    def forward_rows(g, sources):
-        for m in sources:
-            gather[g, m].wait_recv()
-            forward(g, m)
-
-    close, distant = range(1, groups // 2), range(groups // 2, groups)
+            for side in (t, across):
+                send(view, view, 2, wide_r.at[g], (flip(e, m), side))
+        own[g] = send(view, view, 3, own_r.at[g], (e, across))
+
+    def join_rows(g):
+        own[g].wait_recv()
+        arrived(xbuf.at[g, pl.ds(0, 2), pl.ds(0, groups - 1)], wide_r.at[g])
+        for side in (t, across):
+            view = xbuf.at[g, side]
+            send(view, view, 6, join_r.at[g], (e, twin))
 
     for g in range(pieces):
         attention(g)
         if g == 0:
-            pl.semaphore_wait(barrier, parts + groups - 2)
+            pl.semaphore_wait(barrier, parts - 1 + 2 * (groups - 1))
             loads[5].wait()
         send_partials(g)
+        if g == 0:
+            for m in range(groups - 1, 0, -1):
+                send(slot_buf.at[e], slot_buf.at[e], 1, sl_r.at[0], (flip(e, m), t))
         if g >= 1:
             send_rows(g - 1)
-        if g >= 3:
-            forward_rows(g - 3, distant)
-        if g >= 2:
-            forward_rows(g - 2, close)
 
     fetches = loads[6:]
     third = owned
     for load in fetches[:third]:
         load.start()
-    slot_row, later = route_tables(routes_ref[...], logits_ref[...], groups * block, capacity)
-    slot_buf[e] = jnp.broadcast_to(slot_row, (8, n))
-    for m in range(groups - 1, 0, -1):
-        send(slot_buf.at[e], slot_buf.at[e], 1, sl_r.at[0], (flip(e, m), t))
-    share = later()
-    for i in range(3):
-        coarse = share.astype(BF16)
-        combine_v[i * seqs:(i + 1) * seqs, :] = coarse
-        share = share - coarse.astype(F32)
-    forward_rows(last - 2, distant)
+    arrived(slot_buf.at[pl.ds(0, groups - 1)], sl_r.at[0])
+    base = e * block
+    local = (where_is((block, n), 0) + base).astype(F32)
+    chosen = [(slot_buf[b][:1, :] == local).astype(BF16) for b in range(groups)]
+
+    def dispatch_from(first, count):
+        wide_n = count * groups * GROUP
+        token = where_is((n, wide_n), 0) // top
+        spot_row = (token // GROUP - first) * (groups * GROUP) + token % GROUP
+        place = []
+        for b in range(groups):
+            spot = (where_is((n, wide_n), 1) == spot_row + b * GROUP).astype(BF16)
+            placed = jnp.dot(chosen[b], spot, preferred_element_type=F32)
+            place.append(placed.reshape(owned, 1, capacity, wide_n))
+        return jnp.concatenate(place, axis=1).reshape(groups * block, wide_n).astype(BF16)
+
+    def rows_from(first, count, q):
+        rows = xbuf[first:first + count, q].astype(F32)
+        return rows.reshape(count * groups * GROUP, columns).astype(BF16)
+
+    dispatch_first = dispatch_from(0, last)
+    dispatch_v[...] = dispatch_from(last, 1)
     send_rows(last)
     for load in fetches[third:]:
         load.start()
-    for g in range(last - 1):
-        relay_rows(g)
-    forward_rows(last - 1, close)
-    forward_rows(last - 1, distant)
-    forward_rows(last, close)
-    forward_rows(last, distant)
-    arrived(slot_buf.at[pl.ds(0, groups - 1)], sl_r.at[0])
-    base = e * block
-    local = (where_is((block, n), 0) + base).astype(F32)
-    tokens_all = groups * seqs
-    token = where_is((n, tokens_all), 0) // top
-    spot_row = token // GROUP * (groups * GROUP) + token % GROUP
-    place = []
-    for b in range(groups):
-        chosen = (slot_buf[b][:1, :] == local).astype(BF16)
-        spot = (where_is((n, tokens_all), 1) == spot_row + b * GROUP).astype(BF16)
-        placed = jnp.dot(chosen, spot, preferred_element_type=F32)
-        place.append(placed.reshape(owned, 1, capacity, tokens_all))
-    dispatch = jnp.concatenate(place, axis=1).reshape(groups * block, tokens_all).astype(BF16)
-
-    relay_rows(last - 1)
-    relay_rows(last)
-    arrived(xbuf.at[:, 0], near_r.at[0])
-    arrived(xbuf.at[pl.ds(0, last), 0], relay_r.at[0])
-    arrived(xbuf.at[last, 0, pl.ds(0, groups // 2)], relay_r.at[1])
-    for copy in tail.values():
-        copy.wait_recv()
-
-    lines, squares = [], jnp.zeros((groups * block, columns), F32)
+    for g in range(last):
+        join_rows(g)
+    for g in range(last):
+        arrived(xbuf.at[g, pl.ds(0, 2)], join_r.at[g])
     for q in range(parts):
-        rows = xbuf[:, q].astype(F32).reshape(tokens_all, columns).astype(BF16)
-        picked = jnp.dot(dispatch, rows, preferred_element_type=F32)
-        lines.append(picked.astype(BF16))
-        plain = picked * (1.0 / fgain_ref[:, q * columns:(q + 1) * columns])
-        squares = squares + plain * plain
-    lines = jnp.concatenate(lines, axis=-1)
-    mean_sq = jnp.sum(squares, axis=-1, keepdims=True) * (1.0 / (columns * parts))
-    row_scale = lax.rsqrt(mean_sq + EPS)
-    hfar, hnear = [], []
+        lines_v[:, q * columns:(q + 1) * columns] = jnp.dot(
+            dispatch_first, rows_from(0, last, q), preferred_element_type=F32
+        )
+    join_rows(last)
+    arrived(xbuf.at[last, pl.ds(0, 2)], join_r.at[last])
+    late = [rows_from(last, 1, q) for q in range(parts)]
+    unscale = 1.0 / fgain_ref[...]
+    hfar, hnear = [None], [None]
+    half_rows = groups // 2 * capacity
+    home = e // (groups // 2) * (groups // 2)
+    away = groups // 2 - home
     for j in range(owned):
         for i in range(2):
             loads[6 + 3 * j + i].wait()
-        line = lines[j * per:(j + 1) * per]
-        line_scale = row_scale[j * per:(j + 1) * per]
+        picked = jnp.concatenate(
+            [jnp.dot(dispatch_v[j * per:(j + 1) * per, :], rows, preferred_element_type=F32) for rows in late], axis=-1
+        ) + lines_v[j * per:(j + 1) * per, :]
+        line = picked.astype(BF16)
+        plain = picked * unscale
+        mean_sq = jnp.sum(plain * plain, axis=-1, keepdims=True) * (1.0 / (columns * parts))
+        line_scale = lax.rsqrt(mean_sq + EPS)
         gate = jnp.minimum(jnp.dot(line, gate_v[j], preferred_element_type=F32) * line_scale, LIMIT)
         up = jnp.clip(jnp.dot(line, up_v[j], preferred_element_type=F32) * line_scale, -LIMIT, LIMIT)
         hbuf[j, t] = ((up + 1.0) * gate * jax.nn.sigmoid(ALPHA * gate)).astype(BF16)
+        if j == 0:
+            halves = []
+            for i, base_row in enumerate((away, home)):
+                view = hbuf.at[j, t, pl.ds(pl.multiple_of(base_row * capacity, half_rows), half_rows)]
+                halves.append([
+                    send(view, view, 4, hy_r.at[i * owned], (e, across)),
+                    send(view, view, 4, hd_r.at[i * owned], (e, opposite)),
+                    send(view, view, 4, hc_r.at[i * owned], (e, twin)),
+                ])
+            continue
         view = hbuf.at[j, t]
         hfar.append(send(view, view, 4, hy_r.at[j], (e, across)))
-        if j == 0:
-            hrelay = [send(view, view, 4, hd_r.at[j], (e, opposite))]
         hnear.append(send(view, view, 4, hc_r.at[j], (e, twin)))
     deep = hbuf.shape[3]
-    for j in range(owned + 1):
+    hrelay = [None]
+    loads[6 + 2].wait()
+    for i, base_row in enumerate((away, home)):
+        for copy in halves[i]:
+            copy.wait_recv()
+        result = jnp.zeros((half_rows, columns), F32)
+        cut = pl.ds(pl.multiple_of(base_row * capacity, half_rows), half_rows)
+        for q in range(parts):
+            result += jnp.dot(hbuf[0, q, cut, :], down_v[0, q * deep:(q + 1) * deep, :], preferred_element_type=F32)
+        resbuf[0, pl.ds(base_row, groups // 2)] = result.reshape(groups // 2, capacity, columns).astype(BF16)
+        for m in (range(groups - 1, groups // 2 - 1, -1) if i == 0 else range(groups // 2 - 1, 0, -1)):
+            peer = flip(e, m)
+            send(resbuf.at[0, peer], ret.at[e, 0], 5, re_r.at[0], (peer, t))
+    ret[e, 0] = resbuf[0, e]
+    for j in range(1, owned + 1):
         if j < owned:
             hfar[j].wait_recv()
             theirs = hbuf.at[j, across]
-            if j:
-                hrelay.append(send(theirs, theirs, 4, hd_r.at[j], (e, twin)))
-        if j == 0:
+            hrelay.append(send(theirs, theirs, 4, hd_r.at[j], (e, twin)))
+        if j == 1:
             continue
         i = j - 1
         hnear[i].wait_recv()
@@ -657,8 +664,9 @@
     out_ref[...] = (kept[...].reshape(seqs, columns) + moe).astype(out_ref.dtype)
     arrived(part_b.at[:, pl.ds(0, parts - 1)], snd.at[0])
     arrived(slot_buf.at[pl.ds(0, groups - 1)], snd.at[1])
-    arrived(xbuf.at[:, 0, pl.ds(0, groups - 1)], snd.at[2])
-    arrived(xbuf.at[:, pl.ds(0, parts - 1)], snd.at[3])
+    arrived(xbuf.at[:, pl.ds(0, 2), pl.ds(0, groups - 1)], snd.at[2])
+    arrived(xbuf.at[:, 0, 0], snd.at[3])
+    arrived(xbuf.at[:, pl.ds(0, 2)], snd.at[6])
     arrived(hbuf.at[:, pl.ds(0, parts - 1)], snd.at[4])
     arrived(resbuf.at[:, pl.ds(0, groups - 1)], snd.at[5])
 
@@ -700,6 +708,8 @@
         pltpu.VMEM((pieces, GROUP, columns), F32),
         pltpu.VMEM((groups, 8, routes.size), F32),
         pltpu.VMEM((3 * seqs, owned * per), BF16),
+        pltpu.VMEM((owned * per, groups * GROUP), BF16),
+        pltpu.VMEM((owned * per, full), F32),
         pltpu.VMEM((pieces, parts, groups, GROUP, columns), BF16),
         pltpu.VMEM((owned, parts, per, deep), BF16),
         pltpu.VMEM((owned, groups, capacity, columns), BF16),
@@ -707,8 +717,7 @@
     ]
     dma = lambda *shape: [pltpu.SemaphoreType.DMA(shape)]
     scratch += dma(pieces) * 2 + dma(6 + 3 * owned) + dma(8)
-    scratch += dma(6) + dma(pieces) + dma(1) + dma(pieces, groups - 1)
-    scratch += dma(pieces, groups) + dma(1) + dma(2) + dma(groups) + dma(owned) * 3 + dma(1)
+    scratch += dma(7) + dma(pieces) + dma(1) + dma(pieces) * 3 + dma(owned + 1) * 3 + dma(1)
     return pl.pallas_call(
         functools.partial(layer_kernel, heads, groups, parts, capacity),
         out_shape=pltpu.VMEM((seqs, columns), BF16),

time: 44.7 us -> 42 us (0.940)
  Pallas kernels: 43.9 us -> 41.2 us
    pallas_call x1, Pallas kernels: 43.9 us -> 41.2 us  [layer(): pl.pallas_call(functools.partial(layer_kernel, heads, groups, parts, capa...]
where the time goes in v4:
time: 42 us; the launch traced here: 41.8 us
  Pallas kernels  41.2 us (98%)
  local copies, waits for them, and re-layouts  0.62 us (1%)
    pallas_call x1, Pallas kernels, layer(): pl.pallas_call(functools.partial(layer_kernel, heads, groups, parts, capa...  41.2 us

profile of v4, /device:TPU:0, one launch (start us, length us, event | category | flops | bytes accessed | tf_op | source)
XLA Modules:
  0.0 41.8 jit_solution(5655448603411536280)
XLA Ops:
  0.0 41.2 %layer.1 = bf16[32,512]{1,0:T(8,128)(2,1)S(1)} custom-call(f32[2]{0:T(128)} %lam_hbm.1, s32[32]{0:T(128)} %lengths_hbm.1, bf16[32,2048]{1,0:T(8,128)(2,1)} %tokens_hbm.1, f32[1,2048]{1,0:T(1,128)} %bitcast.5, f32[1,128]{1,0:T(1,128)} %bitcast.9, f32[1,2048]{1,0:T(1,128)} %bitcast.6, s32[4,32]{1,0:T(4,128)} %bitcast.7, f32[4,32]{1,0:T(4,128)} %bitcast.8, ...), custom_call_target="tpu_custom_call" | custom-call | tf_op jit(solution)/shard_map/layer/pallas_call | solution.py:721
  41.2 0.6 %copy.21 = bf16[32,512]{1,0:T(8,128)(2,1)} copy(bf16[32,512]{1,0:T(8,128)(2,1)S(1)} %layer.1) | data formatting | bytes 65536
